TPU v7x, 32 devices: a whole 2x2x4 slice. The times are simulated.
32 devices in a mesh: ra: 2 (over core), cb: 4 (over z), dp: 4 (over y, x).
Axes of the slice: x: 2, y: 2, z: 4, core: 2. Of those that a mesh axis runs over, the one named last changes fastest.
Arguments:
- residual_in: bfloat16 [1024, 4096], P('dp', 'cb'), may hold values from -220 to 220, as said below
- gain_in: float32 [4096], P('cb'), may hold values from 0.1 to 1.9
- shift_in: float32 [4096], P('cb'), may hold values from -3 to 3
- up_weight: bfloat16 [4096, 16384], P('cb', 'ra'), may hold values from -0.09375 to 0.09375
- down_weight: bfloat16 [16384, 4096], P('ra', 'cb'), may hold values from -0.046875 to 0.046875
- gain_out: float32 [4096], P('cb'), may hold values from 0.1 to 1.9
- shift_out: float32 [4096], P('cb'), may hold values from -3 to 3
Outputs:
- layer_out: bfloat16 [1024, 4096], P('dp', 'cb')
Inputs may be any that keep to these rules, and one draw needn't show every extreme that they name: `residual_in`: real-valued activations.
All inputs are finite; a program needn't handle non-finite values.
Results may differ from a plain program's by a relative error of at most 0.0065.
Values may be sent and summed in bfloat16 or wider, within the bound.
No kernel may reach another device: no remote copies, remote signals or barrier semaphores. Data moves between devices by JAX's collectives and lax.ppermute only.
A program may use at most 128 MiB of HBM per device.

v0:
```python
import jax
import jax.numpy as jnp
from jax import lax
from jax.sharding import PartitionSpec as P


def standardize(values):
    count = values.shape[1] * lax.axis_size("cb")
    sums = lax.psum(jnp.sum(values, axis=1), "cb")
    mean = sums / count
    centred = values - mean[:, None]
    spread = lax.psum(jnp.sum(centred * centred, axis=1), "cb") / count
    return (values - mean[:, None]) * lax.rsqrt(spread + 1e-05)[:, None]


def per_device(residual_in, gain_in, shift_in, up_weight, down_weight, gain_out, shift_out):
    normed = (standardize(residual_in.astype(jnp.float32)) * gain_in + shift_in).astype(
        jnp.bfloat16
    )
    products = jnp.dot(normed, up_weight, preferred_element_type=jnp.float32)
    share = lax.psum_scatter(products, "cb", scatter_dimension=1, tiled=True)
    hidden_share = jnp.square(jax.nn.relu(share)).astype(jnp.bfloat16)
    branch_part = jnp.dot(
        lax.all_gather(hidden_share, "cb", axis=1, tiled=True),
        down_weight,
        preferred_element_type=jnp.float32,
    )
    branch = lax.psum(branch_part, "ra")
    total = 2.0**0.25 * normed.astype(jnp.float32) + branch
    return (standardize(total) * gain_out + shift_out).astype(jnp.bfloat16)


def solution(mesh):
    in_specs = (P("dp", "cb"), P("cb"), P("cb"), P("cb", "ra"), P("ra", "cb"), P("cb"), P("cb"))
    out_specs = P("dp", "cb")
    return jax.shard_map(
        per_device, mesh=mesh, in_specs=in_specs, out_specs=out_specs, check_vma=False
    )
```

profile of v0, /device:TPU:0, one launch (start us, length us, event | category | flops | bytes accessed | tf_op | source)
XLA Modules:
  0.0 337.2 jit_solution(11542523909155165681)
XLA Ops:
  6.5 0.0 reduce-scatter.2.cloned.1.call-start
  6.5 1.2 convert_reduce_fusion
  7.7 13.5 %psum.35 = f32[256]{0:T(256)S(1)} all-reduce(f32[256]{0:T(256)S(1)} %convert_reduce_fusion), channel_id=1, replica_groups=mesh['ra'=2,'cb'=4,'dp'=4] {'cb'}, use_global_device_ids=true, to_apply=%region_1.0 | all-reduce | flops 256 | bytes 2048 | tf_op jit(solution)/shard_map/psum | solution.py:9
  21.2 1.3 fusion.2
  22.5 8.4 %psum.36 = f32[256]{0:T(256)S(1)} all-reduce(f32[256]{0:T(256)S(1)} %fusion.2), channel_id=1, replica_groups=mesh['ra'=2,'cb'=4,'dp'=4] {'cb'}, use_global_device_ids=true, to_apply=%region_3.0 | all-reduce | flops 256 | bytes 2048 | tf_op jit(solution)/shard_map/psum | solution.py:12
  30.9 13.8 %fusion.7 = f32[256,8192]{1,0:T(8,128)} fusion(bf16[1024,8192]{1,0:T(8,128)(2,1)} %param.10, bf16[256,1024]{1,0:T(8,128)(2,1)} %param.7, f32[1024]{0:T(1024)} %param.9, f32[1024]{0:T(1024)} %param.8, f32[256]{0:T(256)S(1)} %add_rsqrt_fusion.1, f32[256]{0:T(256)S(1)} %broadcast_multiply_fusion.1), kind=kOutput, calls=%fused_computation.17 | convolution fusion | flops 4296540160 | bytes 25700352 | tf_op jit(solution)/shard_map/dot_general | solution.py:20
  44.8 0.0 reduce-scatter.2.cloned.1.call-update
  44.8 0.0 all-gather.2.cloned.1.call-start
  44.8 144.4 %reduce-scatter.2.cloned.1.call-done = f32[256,2048]{1,0:T(8,128)} async-done(((f32[256,8192]{1,0:T(8,128)}), f32[256,2048]{1,0:T(8,128)}) %reduce-scatter.2.cloned.1.call-update) | async-done | bytes 2097168 | tf_op jit(solution)/shard_map/reduce_scatter | solution.py:21
  189.2 2.8 multiply_convert_fusion
  192.0 0.0 all-gather.2.cloned.1.call-update
  192.0 0.0 copy-start
  192.0 0.0 copy-start.1
  192.1 0.0 copy-start.2
  192.1 0.0 copy-start.3
  192.1 0.0 copy-start.4
  192.1 0.0 all-reduce.2.cloned.1.call-start
  192.1 81.4 %all-gather.2.cloned.1.call-done = bf16[256,8192]{1,0:T(8,128)(2,1)} async-done(((bf16[256,2048]{1,0:T(8,128)(2,1)}), bf16[256,8192]{1,0:T(8,128)(2,1)}) %all-gather.2.cloned.1.call-update) | async-done | bytes 4194320 | tf_op jit(solution)/shard_map/all_gather | solution.py:24
  273.5 12.5 %fusion.9 = f32[256,1024]{1,0:T(8,128)} fusion(bf16[256,8192]{1,0:T(8,128)(2,1)} %all-gather.2.cloned.1.call-done, bf16[8192,1024]{1,0:T(8,128)(2,1)} %param.11), kind=kOutput, calls=%fused_computation.18 | convolution fusion | flops 4294967296 | bytes 22020096 | tf_op jit(solution)/shard_map/dot_general | solution.py:23
  286.0 0.0 all-reduce.2.cloned.1.call-update
  286.1 18.1 %all-reduce.2.cloned.1.call-done = f32[256,1024]{1,0:T(8,128)} async-done(((f32[256,1024]{1,0:T(8,128)}), f32[256,1024]{1,0:T(8,128)}) %all-reduce.2.cloned.1.call-update) | async-done | bytes 1048592 | tf_op jit(solution)/shard_map/psum | solution.py:28
  304.1 0.0 copy-done
  304.1 0.0 copy-done.1
  304.1 0.0 copy-done.2
  304.1 1.7 fusion.6
  305.8 12.0 %psum.38 = f32[256]{0:T(256)S(1)} all-reduce(f32[256]{0:T(256)S(1)} %fusion.6), channel_id=1, replica_groups=mesh['ra'=2,'cb'=4,'dp'=4] {'cb'}, use_global_device_ids=true, to_apply=%region_7.8 | all-reduce | flops 256 | bytes 2048 | tf_op jit(solution)/shard_map/psum | solution.py:9
  317.8 1.7 multiply_reduce_fusion
  319.5 8.4 %psum.39 = f32[256]{0:T(256)S(1)} all-reduce(f32[256]{0:T(256)S(1)} %multiply_reduce_fusion), channel_id=1, replica_groups=mesh['ra'=2,'cb'=4,'dp'=4] {'cb'}, use_global_device_ids=true, to_apply=%region_9.10 | all-reduce | flops 256 | bytes 2048 | tf_op jit(solution)/shard_map/psum | solution.py:12
  327.9 0.0 copy-done.3
  327.9 0.0 copy-done.4
  327.9 2.8 add_convert_fusion
  (4 shorter events, 0.0 us)
Async XLA Ops:
  6.5 182.7 %reduce-scatter.2.cloned.1.call-start = ((), (), s32[]{:S(2)}) async-start(), calls=%async_computation.1 | async-start | bytes 10485760 | tf_op jit(solution)/shard_map/reduce_scatter | solution.py:21
  44.8 228.8 %all-gather.2.cloned.1.call-start = ((), (), s32[]{:S(2)}) async-start(), calls=%async_computation.2 | async-start | bytes 5242880 | tf_op jit(solution)/shard_map/all_gather | solution.py:24
  192.0 112.1 %copy-start = (bf16[256,1024]{1,0:T(8,128)(2,1)S(1)}, bf16[256,1024]{1,0:T(8,128)(2,1)}, u32[]{:S(2)}) copy-start(bf16[256,1024]{1,0:T(8,128)(2,1)} %param.7) | copy-start | bytes 1572868
  192.0 112.1 %copy-start.1 = (f32[1024]{0:T(1024)S(1)}, f32[1024]{0:T(1024)}, u32[]{:S(2)}) copy-start(f32[1024]{0:T(1024)} %param.9) | copy-start | bytes 12292
  192.1 112.1 %copy-start.2 = (f32[1024]{0:T(1024)S(1)}, f32[1024]{0:T(1024)}, u32[]{:S(2)}) copy-start(f32[1024]{0:T(1024)} %param.8) | copy-start | bytes 12292
  192.1 135.8 %copy-start.3 = (f32[1024]{0:T(1024)S(1)}, f32[1024]{0:T(1024)}, u32[]{:S(2)}) copy-start(f32[1024]{0:T(1024)} %param.13) | copy-start | bytes 12292
  192.1 135.8 %copy-start.4 = (f32[1024]{0:T(1024)S(1)}, f32[1024]{0:T(1024)}, u32[]{:S(2)}) copy-start(f32[1024]{0:T(1024)} %param.12) | copy-start | bytes 12292
  192.1 112.0 %all-reduce.2.cloned.1.call-start = ((), (), s32[]{:S(2)}) async-start(), calls=%async_computation.3 | async-start | bytes 2097152 | tf_op jit(solution)/shard_map/psum | solution.py:28
Sparse Core Ops, SparseCore 0:
  44.9 144.2 reduce-scatter.1
  192.2 81.3 all-gather.1
  286.2 17.8 all-reduce.1
where the time goes:
time: 338 us; the launch traced here: 337 us
  waiting for transfers between devices  244 us (72%)
  blocking collectives  42.2 us (12%)
  matrix products  26.3 us (8%)
  between operations  13.2 us (4%)
  other arithmetic  11.5 us (3%)
    reduce_scatter x1, waiting for transfers between devices, per_device(): share = lax.psum_scatter(products, 'cb', scatter_dimension=1, tiled=True)  144 us
    all_gather x1, waiting for transfers between devices, per_device(): lax.all_gather(hidden_share, 'cb', axis=1, tiled=True)  81.4 us
    psum x2, blocking collectives, standardize(): sums = lax.psum(jnp.sum(values, axis=1), 'cb')  25.5 us
    psum x1, waiting for transfers between devices, per_device(): branch = lax.psum(branch_part, 'ra')  18.1 us
    psum x2, blocking collectives, standardize(): spread = lax.psum(jnp.sum(centred * centred, axis=1), 'cb') / count  16.7 us
    dot_general x1, matrix products, per_device(): products = jnp.dot(normed, up_weight, preferred_element_type=jnp.float32)  13.8 us
    dot_general x1, matrix products, per_device(): jnp.dot(lax.all_gather(hidden_share, 'cb', axis=1, tiled=True), down_weig...  12.5 us
  transfers between devices with their start and end apart: 3, of which 3 were waited for; matrix products, arithmetic and copies ran while one was open for 0% of the time, Pallas kernels for 0%

commit v1 on v0

--- a/solution.py
+++ b/solution.py
@@ -25,7 +25,8 @@
         down_weight,
         preferred_element_type=jnp.float32,
     )
-    branch = lax.psum(branch_part, "ra")
+    terms = lax.all_gather(branch_part, "ra")
+    branch = jnp.sum(terms, axis=0)
     total = 2.0**0.25 * normed.astype(jnp.float32) + branch
     return (standardize(total) * gain_out + shift_out).astype(jnp.bfloat16)
 

time: 338 us -> 327 us (0.967)
  waiting for transfers between devices: 244 us -> 235 us
    psum x1 -> x0, waiting for transfers between devices: 18.1 us -> none  [per_device(): branch = lax.psum(branch_part, 'ra')]
    all_gather x0 -> x1, waiting for transfers between devices: none -> 9.22 us  [per_device(): terms = lax.all_gather(branch_part, 'ra')]
where the time goes in v1:
time: 327 us
  waiting for transfers between devices  235 us (72%)
  blocking collectives  42.2 us (13%)
  matrix products  26.3 us (8%)
  between operations  13.2 us (4%)
  other arithmetic  9.8 us (3%)
    reduce_scatter x1, waiting for transfers between devices, per_device(): share = lax.psum_scatter(products, 'cb', scatter_dimension=1, tiled=True)  144 us
    all_gather x1, waiting for transfers between devices, per_device(): lax.all_gather(hidden_share, 'cb', axis=1, tiled=True)  81.4 us
    psum x2, blocking collectives, standardize(): sums = lax.psum(jnp.sum(values, axis=1), 'cb')  25.4 us
    psum x2, blocking collectives, standardize(): spread = lax.psum(jnp.sum(centred * centred, axis=1), 'cb') / count  16.7 us
    dot_general x1, matrix products, per_device(): products = jnp.dot(normed, up_weight, preferred_element_type=jnp.float32)  13.8 us
    dot_general x1, matrix products, per_device(): jnp.dot(lax.all_gather(hidden_share, 'cb', axis=1, tiled=True), down_weig...  12.5 us
    all_gather x1, waiting for transfers between devices, per_device(): terms = lax.all_gather(branch_part, 'ra')  9.22 us
  transfers between devices with their start and end apart: 3, of which 3 were waited for; matrix products, arithmetic and copies ran while one was open for 0% of the time, Pallas kernels for 0%

profile of v1, /device:TPU:0, one launch (start us, length us, event | category | flops | bytes accessed | tf_op | source)
XLA Modules:
  0.0 326.7 jit_solution(1673490704276656736)
XLA Ops:
  6.5 0.0 reduce-scatter.2.cloned.1.call-start
  6.5 1.2 convert_reduce_fusion
  7.7 13.5 %psum.28 = f32[256]{0:T(256)S(1)} all-reduce(f32[256]{0:T(256)S(1)} %convert_reduce_fusion), channel_id=1, replica_groups=mesh['ra'=2,'cb'=4,'dp'=4] {'cb'}, use_global_device_ids=true, to_apply=%region_1.0 | all-reduce | flops 256 | bytes 2048 | tf_op jit(solution)/shard_map/psum | solution.py:9
  21.2 1.3 fusion.2
  22.5 8.4 %psum.29 = f32[256]{0:T(256)S(1)} all-reduce(f32[256]{0:T(256)S(1)} %fusion.2), channel_id=1, replica_groups=mesh['ra'=2,'cb'=4,'dp'=4] {'cb'}, use_global_device_ids=true, to_apply=%region_3.0 | all-reduce | flops 256 | bytes 2048 | tf_op jit(solution)/shard_map/psum | solution.py:12
  30.9 13.8 %fusion.7 = f32[256,8192]{1,0:T(8,128)} fusion(bf16[1024,8192]{1,0:T(8,128)(2,1)} %param.10, bf16[256,1024]{1,0:T(8,128)(2,1)} %param.7, f32[1024]{0:T(1024)} %param.9, f32[1024]{0:T(1024)} %param.8, f32[256]{0:T(256)S(1)} %add_rsqrt_fusion.1, f32[256]{0:T(256)S(1)} %broadcast_multiply_fusion.1), kind=kOutput, calls=%fused_computation.17 | convolution fusion | flops 4296540160 | bytes 25700352 | tf_op jit(solution)/shard_map/dot_general | solution.py:20
  44.8 0.0 reduce-scatter.2.cloned.1.call-update
  44.8 0.0 all-gather.4.cloned.1.call-start
  44.8 144.4 %reduce-scatter.2.cloned.1.call-done = f32[256,2048]{1,0:T(8,128)} async-done(((f32[256,8192]{1,0:T(8,128)}), f32[256,2048]{1,0:T(8,128)}) %reduce-scatter.2.cloned.1.call-update) | async-done | bytes 2097168 | tf_op jit(solution)/shard_map/reduce_scatter | solution.py:21
  189.2 2.8 multiply_convert_fusion
  192.0 0.0 all-gather.4.cloned.1.call-update
  192.0 0.0 copy-start
  192.0 0.0 copy-start.1
  192.1 0.0 copy-start.2
  192.1 0.0 copy-start.3
  192.1 0.0 copy-start.4
  192.1 0.0 all-gather.6.cloned.1.call-start
  192.1 81.4 %all-gather.4.cloned.1.call-done = bf16[256,8192]{1,0:T(8,128)(2,1)} async-done(((bf16[256,2048]{1,0:T(8,128)(2,1)}), bf16[256,8192]{1,0:T(8,128)(2,1)}) %all-gather.4.cloned.1.call-update) | async-done | bytes 4194320 | tf_op jit(solution)/shard_map/all_gather | solution.py:24
  273.5 12.5 %fusion.9 = f32[256,1024]{1,0:T(8,128)} fusion(bf16[256,8192]{1,0:T(8,128)(2,1)} %all-gather.4.cloned.1.call-done, bf16[8192,1024]{1,0:T(8,128)(2,1)} %param.11), kind=kOutput, calls=%fused_computation.18 | convolution fusion | flops 4294967296 | bytes 22020096 | tf_op jit(solution)/shard_map/dot_general | solution.py:23
  286.0 0.0 all-gather.6.cloned.1.call-update
  286.1 9.2 %all-gather.6.cloned.1.call-done = f32[512,1024]{1,0:T(8,128)} async-done(((f32[256,1024]{1,0:T(8,128)}), f32[512,1024]{1,0:T(8,128)}) %all-gather.6.cloned.1.call-update) | async-done | bytes 2097168 | tf_op jit(solution)/shard_map/all_gather | solution.py:28
  295.3 1.9 reduce_sum.47
  297.2 0.0 copy-done
  297.2 0.0 copy-done.1
  297.2 0.0 copy-done.2
  297.2 0.5 fusion.6
  297.7 12.0 %psum.30 = f32[256]{0:T(256)S(1)} all-reduce(f32[256]{0:T(256)S(1)} %fusion.6), channel_id=1, replica_groups=mesh['ra'=2,'cb'=4,'dp'=4] {'cb'}, use_global_device_ids=true, to_apply=%region_7.8 | all-reduce | flops 256 | bytes 2048 | tf_op jit(solution)/shard_map/psum | solution.py:9
  309.6 0.5 multiply_reduce_fusion
  310.2 8.4 %psum.31 = f32[256]{0:T(256)S(1)} all-reduce(f32[256]{0:T(256)S(1)} %multiply_reduce_fusion), channel_id=1, replica_groups=mesh['ra'=2,'cb'=4,'dp'=4] {'cb'}, use_global_device_ids=true, to_apply=%region_9.10 | all-reduce | flops 256 | bytes 2048 | tf_op jit(solution)/shard_map/psum | solution.py:12
  318.6 0.0 copy-done.3
  318.6 0.0 copy-done.4
  318.6 1.6 add_convert_fusion
  (4 shorter events, 0.0 us)
Async XLA Ops:
  6.5 182.7 %reduce-scatter.2.cloned.1.call-start = ((), (), s32[]{:S(2)}) async-start(), calls=%async_computation.1 | async-start | bytes 10485760 | tf_op jit(solution)/shard_map/reduce_scatter | solution.py:21
  44.8 228.8 %all-gather.4.cloned.1.call-start = ((), (), s32[]{:S(2)}) async-start(), calls=%async_computation.2 | async-start | bytes 5242880 | tf_op jit(solution)/shard_map/all_gather | solution.py:24
  192.0 105.1 %copy-start = (bf16[256,1024]{1,0:T(8,128)(2,1)S(1)}, bf16[256,1024]{1,0:T(8,128)(2,1)}, u32[]{:S(2)}) copy-start(bf16[256,1024]{1,0:T(8,128)(2,1)} %param.7) | copy-start | bytes 1572868
  192.0 105.1 %copy-start.1 = (f32[1024]{0:T(1024)S(1)}, f32[1024]{0:T(1024)}, u32[]{:S(2)}) copy-start(f32[1024]{0:T(1024)} %param.9) | copy-start | bytes 12292
  192.1 105.1 %copy-start.2 = (f32[1024]{0:T(1024)S(1)}, f32[1024]{0:T(1024)}, u32[]{:S(2)}) copy-start(f32[1024]{0:T(1024)} %param.8) | copy-start | bytes 12292
  192.1 126.5 %copy-start.3 = (f32[1024]{0:T(1024)S(1)}, f32[1024]{0:T(1024)}, u32[]{:S(2)}) copy-start(f32[1024]{0:T(1024)} %param.13) | copy-start | bytes 12292
  192.1 126.5 %copy-start.4 = (f32[1024]{0:T(1024)S(1)}, f32[1024]{0:T(1024)}, u32[]{:S(2)}) copy-start(f32[1024]{0:T(1024)} %param.12) | copy-start | bytes 12292
  192.1 103.2 %all-gather.6.cloned.1.call-start = ((), (), s32[]{:S(2)}) async-start(), calls=%async_computation.3 | async-start | bytes 3145728 | tf_op jit(solution)/shard_map/all_gather | solution.py:28
Sparse Core Ops, SparseCore 0:
  44.9 144.2 reduce-scatter.1
  192.2 81.3 all-gather.3
  286.2 9.0 all-gather.5
